TPU v7x, 128 devices: a whole 4x4x4 slice. The times are simulated.
128 devices in a mesh: sp: 16 (over z, y), dp: 8 (over x, core).
Axes of the slice: x: 4, y: 4, z: 4, core: 2. Of those that a mesh axis runs over, the one named last changes fastest.
Arguments:
- inputs: bfloat16 [8, 3072, 2048], P('dp', 'sp'), may hold values from -6 to 6
- in_gain: float32 [2048], replicated, may hold values from 0.1 to 1.9
- w_query: bfloat16 [2048, 1024], P('dp', 'sp'), may hold values from -0.125 to 0.125
- w_key: bfloat16 [2048, 256], P('dp', 'sp'), may hold values from -0.375 to 0.375
- w_value: bfloat16 [2048, 256], P('dp', 'sp'), may hold values from -0.125 to 0.125
- key_bias: float32 [8, 3072, 16], P('dp', None, 'sp'), may hold values from -20 to 0
- out_gain: float32 [1024], replicated, may hold values from 0.1 to 1.9
- w_out: bfloat16 [1024, 2048], P('sp', 'dp'), may hold values from -0.1875 to 0.1875
Outputs:
- mixed: bfloat16 [8, 3072, 2048], P('dp', 'sp')
All inputs are finite; a program needn't handle non-finite values.
Results may differ from a plain program's by a relative error of at most 0.012.
The roundings to bfloat16 on the way count: a program that leaves them out, or rounds other values in their place, can miss the bound.
Values may be sent and summed in bfloat16 or wider, within the bound.
A program may use at most 128 MiB of HBM per device.

v0:
```python
import jax
import jax.numpy as jnp
from jax import lax
from jax.sharding import PartitionSpec as P

HEAD_DIM = 64
norm_eps = 1e-06


def rows_first(arrays, axis, dims):
    turned = [jnp.moveaxis(a, dim, 0) for a, dim in zip(arrays, dims)]
    both = jnp.concatenate([t.reshape(len(t), -1) for t in turned], axis=1)
    whole, at, finished = (lax.all_gather(both, axis, axis=0, tiled=True), 0, [])
    for t, dim in zip(turned, dims):
        slab = whole[:, at : at + t[0].size].reshape(-1, *t.shape[1:])
        finished.append(jnp.moveaxis(slab, 0, dim))
        at += t[0].size
    return tuple(finished)


def sent_together(arrays, axis, split_dim, concat_dim, along):
    ends, at = ([], 0)
    for a in arrays[:-1]:
        at += a.shape[along]
        ends.append(at)
    both = jnp.concatenate(arrays, axis=along)
    return tuple(
        jnp.split(
            lax.all_to_all(both, axis, split_axis=split_dim, concat_axis=concat_dim, tiled=True),
            ends,
            axis=along,
        )
    )


def body(inputs, in_gain, w_query, w_key, w_value, key_bias, out_gain, w_out):
    width_sp = lax.axis_size("sp")
    own_index = lax.axis_index("sp")
    wide = inputs[0].astype(jnp.float32)
    normed_rows = (
        wide * lax.rsqrt(jnp.mean(wide * wide, axis=-1, keepdims=True) + norm_eps) * in_gain
    ).astype(jnp.bfloat16)
    local_rows = normed_rows.shape[0]
    w_query, w_key, w_value, w_out = rows_first(
        (w_query, w_key, w_value, w_out), "dp", (0, 0, 0, 1)
    )
    w_key, w_value = rows_first((w_key, w_value), "sp", (1, 1))
    keys = jnp.dot(normed_rows, w_key, preferred_element_type=jnp.float32).astype(jnp.bfloat16)
    values = jnp.dot(normed_rows, w_value, preferred_element_type=jnp.float32).astype(jnp.bfloat16)
    queries = jnp.dot(
        normed_rows,
        lax.all_gather(w_query, "sp", axis=1, tiled=True),
        preferred_element_type=jnp.float32,
    ).astype(jnp.bfloat16)
    heads_here = key_bias.shape[2]
    kv_heads = keys.shape[1] // HEAD_DIM
    spread = width_sp // kv_heads
    query_slots = queries.reshape(local_rows, width_sp, heads_here * HEAD_DIM)
    key_copies = jnp.repeat(keys.reshape(local_rows, kv_heads, HEAD_DIM), spread, axis=1)
    value_copies = jnp.repeat(values.reshape(local_rows, kv_heads, HEAD_DIM), spread, axis=1)
    query_all, key_all, value_all = sent_together(
        (query_slots, key_copies, value_copies), "sp", 1, 0, 2
    )
    keys_head = key_all[:, 0, :]
    values_head = value_all[:, 0, :]
    length_all = query_all.shape[0]
    bias_here = key_bias[0].T
    block = min(512, length_all)
    pieces = []
    for index in range(length_all // block):
        start = index * block
        end = start + block
        logits = jnp.einsum(
            "thd,sd->hts", query_all[start:end], keys_head[:end], preferred_element_type=jnp.float32
        )
        logits = logits * HEAD_DIM ** (-0.5) + bias_here[:, None, :end]
        rows = start + jnp.arange(block, dtype=jnp.int32)[:, None]
        columns = jnp.arange(end, dtype=jnp.int32)[None, :]
        strict = (columns < rows)[None, :, :]
        log_keep = jnp.where(strict, jax.nn.log_sigmoid(-logits), jnp.float32(0.0))
        log_rest = lax.cumsum(log_keep, axis=2, reverse=True) - log_keep
        sticks = jnp.where(
            strict, jnp.exp(jax.nn.log_sigmoid(logits) + log_rest), jnp.float32(0.0)
        ).astype(jnp.bfloat16)
        pieces.append(
            jnp.einsum("hts,sd->thd", sticks, values_head[:end], preferred_element_type=jnp.float32)
        )
    attended = jnp.concatenate(pieces, axis=0)
    gains = lax.dynamic_slice_in_dim(
        out_gain, own_index * heads_here * HEAD_DIM, heads_here * HEAD_DIM, 0
    )
    scaled = attended * lax.rsqrt(jnp.mean(attended * attended, axis=-1, keepdims=True) + norm_eps)
    head_out = (scaled * gains.reshape(heads_here, HEAD_DIM)).astype(jnp.bfloat16)
    returned = lax.all_to_all(head_out, "sp", split_axis=0, concat_axis=1, tiled=True)
    returned = returned.reshape(local_rows, width_sp * heads_here * HEAD_DIM)
    mixed = jnp.dot(
        returned,
        lax.all_gather(w_out, "sp", axis=0, tiled=True),
        preferred_element_type=jnp.float32,
    )
    return mixed.astype(jnp.bfloat16)[None]


def solution(mesh):
    placed = (
        P("dp", "sp", None),
        P(),
        P("dp", "sp"),
        P("dp", "sp"),
        P("dp", "sp"),
        P("dp", None, "sp"),
        P(),
        P("sp", "dp"),
    )
    return jax.shard_map(
        body, mesh=mesh, in_specs=placed, out_specs=P("dp", "sp", None), check_vma=False
    )
```

profile of v0, /device:TPU:0, one launch (start us, length us, event | category | flops | bytes accessed | tf_op | source)
XLA Modules:
  0.0 349.7 jit_solution(17781443614021492482)
XLA Ops:
  6.5 0.9 pad_maximum_fusion.2
  7.4 13.7 %all_gather.12 = bf16[2048,160]{0,1:T(8,128)(2,1)S(1)} all-gather(bf16[256,160]{0,1:T(8,128)(2,1)S(1)} %pad_maximum_fusion.2), channel_id=1, replica_groups=mesh['sp'=16,'dp'=8] {'dp'}, dimensions={0}, use_global_device_ids=true | all-gather | bytes 737280 | tf_op jit(solution)/shard_map/all_gather | solution.py:13
  21.1 0.7 pad_maximum_fusion.1
  21.9 0.8 slice_bitcast_fusion.8
  23.0 45.8 %all-gather.6.cloned.1.call-done = bf16[256,4096]{1,0:T(8,128)(2,1)} async-done(((bf16[16,4096]{1,0:T(8,128)(2,1)}), bf16[256,4096]{1,0:T(8,128)(2,1)}) %all-gather.6.cloned.1.call-update) | async-done | bytes 2097168 | tf_op jit(solution)/shard_map/all_gather | solution.py:13
  68.8 1.9 convolution_convert_fusion.2
  71.4 50.3 %all-gather.4.cloned.1.call-done = bf16[2048,1024]{0,1:T(8,128)(2,1)} async-done(((bf16[2048,64]{0,1:T(8,128)(2,1)}), bf16[2048,1024]{0,1:T(8,128)(2,1)}) %all-gather.4.cloned.1.call-update) | async-done | bytes 4194320 | tf_op jit(solution)/shard_map/all_gather | solution.py:52
  121.7 3.7 %convolution_convert_fusion.1 = bf16[192,1024]{1,0:T(8,128)(2,1)S(1)} fusion(bf16[2048,1024]{0,1:T(8,128)(2,1)} %all-gather.4.cloned.1.call-done, bf16[1,192,2048]{2,1,0:T(8,128)(2,1)S(1)} %copy-done.4, f32[2048]{0:T(1024)S(1)} %copy-done.7, f32[192]{0:T(256)S(1)} %add_rsqrt_fusion.1), kind=kOutput, calls=%fused_computation.128 | convolution fusion | flops 807075840 | bytes 5382912 | tf_op jit(solution)/shard_map/dot_general | solution.py:50
  125.8 1.4 pad_maximum_fusion
  127.2 5.3 %all-to-all-start = ((bf16[192,16,192]{0,2,1:T(8,128)(2,1)}), bf16[192,16,192]{0,2,1:T(8,128)(2,1)S(1)}, u32[]{:S(2)}, u32[]{:S(2)}) async-start(bf16[192,16,192]{0,2,1:T(8,128)(2,1)} %pad_maximum_fusion), calls=%async_computation | async-start | bytes 3145728 | tf_op jit(solution)/shard_map/all_to_all | solution.py:29
  132.5 0.6 all-gather.8.cloned.1.call-start
  133.3 0.8 dynamic_slice.3
  134.2 23.7 %all-to-all-done = bf16[192,16,192]{0,2,1:T(8,128)(2,1)S(1)} async-done(((bf16[192,16,192]{0,2,1:T(8,128)(2,1)}), bf16[192,16,192]{0,2,1:T(8,128)(2,1)S(1)}, u32[]{:S(2)}, u32[]{:S(2)}) %all-to-all-start) | async-done | bytes 1179680 | tf_op jit(solution)/shard_map/all_to_all | solution.py:29
  157.9 0.9 copy.59
  158.7 1.7 all_to_all.27
  160.5 1.6 fusion.116
  162.1 4.8 %fusion.121 = f32[1,512,4,128]{1,2,3,0:T(4,128)S(1)} fusion(f32[1,512,4,128]{1,3,2,0:T(8,128)S(1)} %bitcast.409), kind=kOutput, calls=%fused_computation.155 | output fusion | flops 33292288 | bytes 2097152 | tf_op jit(solution)/shard_map/reduce-window
  166.9 1.3 copy.61
  168.2 2.9 fusion.66
  171.0 5.2 %fusion.74 = f32[1,512,8,128]{1,2,3,0:T(8,128)S(1)} fusion(f32[1,512,8,128]{1,3,2,0:T(8,128)S(1)} %bitcast.404), kind=kOutput, calls=%fused_computation.113 | output fusion | flops 66584576 | bytes 4194304 | tf_op jit(solution)/shard_map/reduce-window.2
  176.2 2.6 copy.63
  178.8 4.1 %fusion.53 = (f32[1,512,1536]{1,2,0:T(8,128)S(1)}, f32[1,512,1536]{1,2,0:T(8,128)}) fusion(s32[512]{0:T(512)S(1)} %iota_add_fusion.3, f32[1536]{0:T(1024)S(1)} %slice_reduce_fusion.1, bf16[3072,1,192]{0,2,1:T(8,128)(2,1)S(1)} %all_to_all.27), kind=kOutput, calls=%fused_computation.82 | convolution fusion | flops 109314048 | bytes 6563840 | tf_op jit(solution)/shard_map/thd,sd->hts/dot_general | solution.py:73
  182.9 10.1 %fusion.42 = f32[1,512,12,128]{1,2,3,0:T(8,128)S(1)} fusion(f32[1,512,12,128]{1,3,2,0:T(8,128)S(1)} %bitcast.402), kind=kOutput, calls=%fused_computation.69 | output fusion | flops 99876864 | bytes 6291456 | tf_op jit(solution)/shard_map/reduce-window.4
  193.0 1.8 copy.65
  194.9 6.1 %fusion.34 = (f32[1,512,2048]{1,2,0:T(8,128)S(1)}, f32[2048,512]{1,0:T(8,128)}) fusion(f32[2048]{0:T(1024)S(1)} %bitcast.419, s32[512]{0:T(512)S(1)} %iota_add_fusion.2, bf16[3072,1,192]{0,2,1:T(8,128)(2,1)} %copy-done.1), kind=kOutput, calls=%fused_computation.56 | convolution fusion | flops 145752064 | bytes 8726528 | tf_op jit(solution)/shard_map/thd,sd->hts/dot_general | solution.py:73
  201.0 10.3 %fusion.40 = f32[1,512,16,128]{1,2,3,0:T(8,128)S(1)} fusion(f32[1,512,16,128]{1,3,2,0:T(8,128)S(1)} %bitcast.401), kind=kOutput, calls=%fused_computation.67 | output fusion | flops 133169152 | bytes 8388608 | tf_op jit(solution)/shard_map/reduce-window.6
  211.3 4.4 %copy.67 = f32[1,512,16,128]{1,3,2,0:T(8,128)} copy(f32[1,512,16,128]{1,2,3,0:T(8,128)S(1)} %fusion.40) | data formatting | bytes 8388608 | tf_op jit(solution)/shard_map/reduce-window.6
  215.8 7.1 %fusion.22 = (f32[1,512,2560]{1,2,0:T(8,128)S(1)}, f32[2560,512,1]{1,0,2:T(8,128)}) fusion(s32[512]{0:T(512)S(1)} %iota_add_fusion.1, f32[2560]{0:T(1024)S(1)} %slice_reduce_fusion, bf16[3072,1,192]{0,2,1:T(8,128)(2,1)} %copy-done.1), kind=kOutput, calls=%fused_computation.38 | convolution fusion | flops 182190080 | bytes 10891264 | tf_op jit(solution)/shard_map/thd,sd->hts/dot_general | solution.py:73
  222.9 15.6 %fusion.14 = f32[1,512,20,128]{1,2,3,0:T(8,128)S(1)} fusion(f32[1,512,20,128]{1,3,2,0:T(8,128)S(1)} %bitcast.400), kind=kOutput, calls=%fused_computation.27 | output fusion | flops 166461440 | bytes 10485760 | tf_op jit(solution)/shard_map/reduce-window.8
  238.5 5.4 %copy.69 = f32[1,512,20,128]{1,3,2,0:T(8,128)} copy(f32[1,512,20,128]{1,2,3,0:T(8,128)S(1)} %fusion.14) | data formatting | bytes 10485760 | tf_op jit(solution)/shard_map/reduce-window.8
  244.0 8.2 %fusion.6 = (f32[1,512,3072]{1,2,0:T(8,128)S(1)}, f32[3072,512]{1,0:T(8,128)}) fusion(f32[3072]{0:T(1024)S(1)} %bitcast.417, s32[512]{0:T(512)S(1)} %iota_add_fusion, bf16[3072,1,192]{0,2,1:T(8,128)(2,1)} %copy-done.1), kind=kOutput, calls=%fused_computation.14 | convolution fusion | flops 218628096 | bytes 13056000 | tf_op jit(solution)/shard_map/thd,sd->hts/dot_general | solution.py:73
  252.2 15.3 %fusion.12 = f32[1,512,24,128]{1,2,3,0:T(8,128)S(1)} fusion(f32[1,512,24,128]{1,3,2,0:T(8,128)S(1)} %bitcast.398), kind=kOutput, calls=%fused_computation.25 | output fusion | flops 199753728 | bytes 12582912 | tf_op jit(solution)/shard_map/reduce-window.10
  267.5 6.3 %copy.71 = f32[1,512,24,128]{1,3,2,0:T(8,128)} copy(f32[1,512,24,128]{1,2,3,0:T(8,128)S(1)} %fusion.12) | data formatting | bytes 12582912 | tf_op jit(solution)/shard_map/reduce-window.10
  274.0 2.6 fusion.114
  276.7 5.8 %fusion.64 = bf16[1,512,1024]{1,2,0:T(8,128)(2,1)S(1)} fusion(f32[1,512,8,128]{1,3,2,0:T(8,128)} %copy.63, f32[1024,512]{1,0:T(8,128)} %get-tuple-element.12, f32[512,8]{0,1:T(8,128)S(1)} %slice_bitcast_fusion.47, f32[1024]{0:T(1024)S(1)} %bitcast.423, s32[512]{0:T(512)S(1)} %iota_add_fusion.4), kind=kLoop, calls=%fused_computation.98 | loop fusion | flops 12582912 | bytes 5265408 | tf_op jit(solution)/shard_map/convert_element_type | solution.py:84
  282.5 6.4 %fusion.51 = bf16[1,512,1536]{1,2,0:T(8,128)(2,1)S(1)} fusion(f32[1,512,12,128]{1,3,2,0:T(8,128)S(1)} %copy.65, f32[1,512,1536]{1,2,0:T(8,128)} %get-tuple-element.14, f32[512,12]{0,1:T(8,128)S(1)} %slice_bitcast_fusion.45, s32[512]{0:T(512)S(1)} %iota_add_fusion.3), kind=kLoop, calls=%fused_computation.80 | loop fusion | flops 17301504 | bytes 7890944 | tf_op jit(solution)/shard_map/convert_element_type | solution.py:84
  288.9 7.3 %fusion.32 = bf16[1,512,2048]{1,2,0:T(8,128)(2,1)S(1)} fusion(f32[1,512,16,128]{1,3,2,0:T(8,128)S(1)} %copy-done, f32[2048,512]{1,0:T(8,128)S(1)} %copy-done.3, f32[512,16]{0,1:T(8,128)S(1)} %slice_bitcast_fusion.43, f32[2048]{0:T(1024)S(1)} %bitcast.420, s32[512]{0:T(512)S(1)} %iota_add_fusion.2), kind=kLoop, calls=%fused_computation.54 | loop fusion | flops 25165824 | bytes 10528768 | tf_op jit(solution)/shard_map/convert_element_type | solution.py:84
  296.3 9.8 %fusion.20 = bf16[1,512,2560]{1,2,0:T(8,128)(2,1)S(1)} fusion(f32[1,512,20,128]{1,3,2,0:T(8,128)S(1)} %bitcast.395, f32[2560,512,1]{1,0,2:T(8,128)} %get-tuple-element.18, f32[512,20]{0,1:T(8,128)S(1)} %slice_bitcast_fusion.41, s32[512]{0:T(512)S(1)} %iota_add_fusion.1), kind=kLoop, calls=%fused_computation.36 | loop fusion | flops 28835840 | bytes 13150208 | tf_op jit(solution)/shard_map/convert_element_type | solution.py:84
  306.2 10.9 %fusion.4 = bf16[1,512,3072]{1,2,0:T(8,128)(2,1)S(1)} fusion(f32[1,512,24,128]{1,3,2,0:T(8,128)S(1)} %bitcast.393, f32[3072,512]{1,0:T(8,128)S(1)} %bitcast.397, f32[512,24]{0,1:T(8,128)S(1)} %slice_bitcast_fusion.39, f32[3072]{0:T(1024)S(1)} %bitcast.418, s32[512]{0:T(512)S(1)} %iota_add_fusion), kind=kLoop, calls=%fused_computation.12 | loop fusion | flops 37748736 | bytes 15792128 | tf_op jit(solution)/shard_map/convert_element_type | solution.py:84
  318.5 0.6 fusion.93
  319.0 0.7 fusion.107
  319.9 0.6 broadcast.275
  320.5 0.9 reduce.5
  322.4 13.3 %all_to_all.33 = bf16[16,2,6144]{2,1,0:T(2,128)(2,1)S(1)} all-to-all(bf16[16,2,6144]{2,1,0:T(2,128)(2,1)S(1)} %reshape.777), channel_id=1, replica_groups=mesh['sp'=16,'dp'=8] {'sp'}, dimensions={0} | all-to-all | bytes 786432 | tf_op jit(solution)/shard_map/all_to_all | solution.py:94
  335.7 0.8 reshape.778
  336.5 1.5 copy.73
  338.0 0.6 all_to_all.29
  338.8 4.1 %fusion.59 = bf16[1,192,2048]{2,1,0:T(8,128)(2,1)} fusion(bf16[192,1024]{0,1:T(8,128)(2,1)S(1)} %bitcast.408, bf16[1024,2048]{1,0:T(8,128)(2,1)} %all-gather.8.cloned.1.call-done), kind=kOutput, calls=%fused_computation.93 | convolution fusion | flops 805699584 | bytes 5373952 | tf_op jit(solution)/shard_map/dot_general | solution.py:96
  (84 shorter events, 4.9 us)
Async XLA Ops:
  6.5 16.2 %copy-start.4 = (bf16[1,192,2048]{2,1,0:T(8,128)(2,1)S(1)}, bf16[1,192,2048]{2,1,0:T(8,128)(2,1)}, u32[]{:S(2)}) copy-start(bf16[1,192,2048]{2,1,0:T(8,128)(2,1)} %param.8) | copy-start | bytes 2359300
  6.5 62.3 %copy-start.7 = (f32[2048]{0:T(1024)S(1)}, f32[2048]{0:T(1024)}, u32[]{:S(2)}) copy-start(f32[2048]{0:T(1024)} %param.9) | copy-start | bytes 24580
  6.5 62.2 %all-gather.6.cloned.1.call-start = ((), (), s32[]{:S(2)}) async-start(), calls=%async_computation.3 | async-start | bytes 2228224 | tf_op jit(solution)/shard_map/all_gather | solution.py:13
  21.8 99.9 %all-gather.4.cloned.1.call-start = ((), (), s32[]{:S(2)}) async-start(), calls=%async_computation.2 | async-start | bytes 4456448 | tf_op jit(solution)/shard_map/all_gather | solution.py:52
  68.8 2.0 copy-start.6
  125.8 7.5 %copy-start.5 = (f32[1,3072,1]{1,2,0:T(1,128)S(1)}, f32[1,3072,1]{1,2,0:T(1,128)}, u32[]{:S(2)}) copy-start(f32[1,3072,1]{1,2,0:T(1,128)} %param.13) | copy-start | bytes 36868
  127.2 30.6 %all-to-all-start = ((bf16[192,16,192]{0,2,1:T(8,128)(2,1)}), bf16[192,16,192]{0,2,1:T(8,128)(2,1)S(1)}, u32[]{:S(2)}, u32[]{:S(2)}) async-start(bf16[192,16,192]{0,2,1:T(8,128)(2,1)} %pad_maximum_fusion), calls=%async_computation | async-start | bytes 3145728 | tf_op jit(solution)/shard_map/all_to_all | solution.py:29
  132.5 206.2 %all-gather.8.cloned.1.call-start = ((), (), s32[]{:S(2)}) async-start(), calls=%async_computation.4 | async-start | bytes 4456448 | tf_op jit(solution)/shard_map/all_gather | solution.py:98
  160.4 18.4 %copy-start.1 = (bf16[3072,1,192]{0,2,1:T(8,128)(2,1)}, bf16[3072,1,192]{0,2,1:T(8,128)(2,1)S(1)}, u32[]{:S(2)}) copy-start(bf16[3072,1,192]{0,2,1:T(8,128)(2,1)S(1)} %all_to_all.27) | copy-start | bytes 3538948
  274.0 14.8 %copy-start.3 = (f32[2048,512]{1,0:T(8,128)S(1)}, f32[2048,512]{1,0:T(8,128)}, u32[]{:S(2)}) copy-start(f32[2048,512]{1,0:T(8,128)} %get-tuple-element.16) | copy-start | bytes 12582916
  276.7 19.6 %slice-start.2 = ((s8[5242880]{0:T(1024)(128)(4,1)}), s8[4194304]{0:T(1024)(128)(4,1)S(1)}, s32[]{:S(2)}) async-start(s8[5242880]{0:T(1024)(128)(4,1)} %bitcast.394), calls=%async_computation.7 | async-start | bytes 8388608
  282.4 6.4 %copy-start = (f32[1,512,16,128]{1,3,2,0:T(8,128)S(1)}, f32[1,512,16,128]{1,3,2,0:T(8,128)}, u32[]{:S(2)}) copy-start(f32[1,512,16,128]{1,3,2,0:T(8,128)} %copy.67) | copy-start | bytes 12582916
  282.4 13.8 %slice-start.3 = ((s8[5242880]{0:T(1024)(128)(4,1)}), s8[1048576]{0:T(1024)(128)(4,1)S(1)}, s32[]{:S(2)}) async-start(s8[5242880]{0:T(1024)(128)(4,1)} %bitcast.394), calls=%async_computation.8 | async-start | bytes 2097152
  288.9 17.3 %slice-start = ((s8[6291456]{0:T(1024)(128)(4,1)}), s8[4194304]{0:T(1024)(128)(4,1)S(1)}, s32[]{:S(2)}) async-start(s8[6291456]{0:T(1024)(128)(4,1)} %bitcast.392), calls=%async_computation.5 | async-start | bytes 8388608
  288.9 17.3 %slice-start.4 = ((s8[6291456]{0:T(1024)(128)(4,1)}), s8[2097152]{0:T(1024)(128)(4,1)S(1)}, s32[]{:S(2)}) async-start(s8[6291456]{0:T(1024)(128)(4,1)} %bitcast.396), calls=%async_computation.9 | async-start | bytes 4194304
  296.2 9.9 %slice-start.1 = ((s8[6291456]{0:T(1024)(128)(4,1)}), s8[2097152]{0:T(1024)(128)(4,1)S(1)}, s32[]{:S(2)}) async-start(s8[6291456]{0:T(1024)(128)(4,1)} %bitcast.392), calls=%async_computation.6 | async-start | bytes 4194304
  296.2 9.9 %slice-start.5 = ((s8[6291456]{0:T(1024)(128)(4,1)}), s8[4194304]{0:T(1024)(128)(4,1)S(1)}, s32[]{:S(2)}) async-start(s8[6291456]{0:T(1024)(128)(4,1)} %bitcast.396), calls=%async_computation.10 | async-start | bytes 8388608
  306.2 10.9 %copy-start.2 = (bf16[3072,1,192]{0,2,1:T(8,128)(2,1)S(1)}, bf16[3072,1,192]{0,2,1:T(8,128)(2,1)}, u32[]{:S(2)}) copy-start(bf16[3072,1,192]{0,2,1:T(8,128)(2,1)} %copy-done.1) | copy-start | bytes 3538948
Sparse Core Ops, SparseCore 0:
  21.9 46.8 all-gather.5
  70.9 50.7 all-gather.3
  135.5 54.9 all-gather.7
where the time goes:
time: 353 us; the launch traced here: 350 us
  waiting for transfers between devices  120 us (34%)
  other arithmetic  109 us (31%)
  matrix products  42.7 us (12%)
  local copies, waits for them, and re-layouts  31.2 us (9%)
  blocking collectives  27 us (8%)
  between operations  14 us (4%)
  starting transfers between devices  5.9 us (2%)
    another operation x12, other arithmetic  61.8 us
    all_gather x1, waiting for transfers between devices, body(): lax.all_gather(w_query, 'sp', axis=1, tiled=True)  50.3 us
    all_gather x1, waiting for transfers between devices, rows_first(): lax.all_gather(both, axis, axis=0, tiled=True)  45.8 us
    convert_element_type x6, other arithmetic, body(): sticks = jnp.where(strict, jnp.exp(jax.nn.log_sigmoid(logits) + log_rest)...  42.8 us
    dot_general x6, matrix products, body(): jnp.einsum('thd,sd->hts', query_all[start:end], keys_head[:end], preferre...  29.9 us
    all_to_all x1, waiting for transfers between devices, sent_together(): lax.all_to_all(both, axis, split_axis=split_dim, concat_axis=concat_dim,...  23.7 us
    another operation x18, local copies, waits for them, and re-layouts  21.8 us
    all_gather x1, blocking collectives, rows_first(): lax.all_gather(both, axis, axis=0, tiled=True)  13.7 us
  transfers between devices with their start and end apart: 4, of which 3 were waited for; matrix products, arithmetic and copies ran while one was open for 48% of the time, Pallas kernels for 0%

commit v1 on v0

--- a/solution.py
+++ b/solution.py
@@ -49,7 +49,7 @@
     values = jnp.dot(normed_rows, w_value, preferred_element_type=jnp.float32).astype(jnp.bfloat16)
     queries = jnp.dot(
         normed_rows,
-        lax.all_gather(w_query, "sp", axis=1, tiled=True),
+        jnp.concatenate(lax.all_gather(w_query, "sp"), axis=1),
         preferred_element_type=jnp.float32,
     ).astype(jnp.bfloat16)
     heads_here = key_bias.shape[2]

time: 353 us -> 362 us (1.025); the launches traced: 350 us -> 355 us
  local copies, waits for them, and re-layouts: 31.2 us -> 38.1 us
    unnamed x31 -> x32, local copies, waits for them, and re-layouts: 1.76 us -> 6.35 us
where the time goes in v1:
time: 362 us; the launch traced here: 355 us
  waiting for transfers between devices  120 us (33%)
  other arithmetic  109 us (30%)
  matrix products  40.5 us (11%)
  local copies, waits for them, and re-layouts  38.1 us (11%)
  blocking collectives  27 us (7%)
  between operations  14.2 us (4%)
  starting transfers between devices  5.59 us (2%)
    another operation x12, other arithmetic  61.9 us
    all_gather x1, waiting for transfers between devices, body(): lax.all_gather(w_query, 'sp')  50.3 us
    all_gather x1, waiting for transfers between devices, rows_first(): lax.all_gather(both, axis, axis=0, tiled=True)  45.8 us
    convert_element_type x6, other arithmetic, body(): sticks = jnp.where(strict, jnp.exp(jax.nn.log_sigmoid(logits) + log_rest)...  42.8 us
    dot_general x6, matrix products, body(): jnp.einsum('thd,sd->hts', query_all[start:end], keys_head[:end], preferre...  29.9 us
    all_to_all x1, waiting for transfers between devices, sent_together(): lax.all_to_all(both, axis, split_axis=split_dim, concat_axis=concat_dim,...  23.7 us
    another operation x18, local copies, waits for them, and re-layouts  21.8 us
    all_gather x1, blocking collectives, rows_first(): lax.all_gather(both, axis, axis=0, tiled=True)  13.7 us
  transfers between devices with their start and end apart: 4, of which 3 were waited for; matrix products, arithmetic and copies ran while one was open for 48% of the time, Pallas kernels for 0%

profile of v1, /device:TPU:0, one launch (start us, length us, event | category | flops | bytes accessed | tf_op | source)
XLA Modules:
  0.0 354.7 jit_solution(16924949615118615228)
XLA Ops:
  6.5 0.9 pad_maximum_fusion.2
  7.4 13.7 %all_gather.15 = bf16[2048,160]{0,1:T(8,128)(2,1)S(1)} all-gather(bf16[256,160]{0,1:T(8,128)(2,1)S(1)} %pad_maximum_fusion.2), channel_id=1, replica_groups=mesh['sp'=16,'dp'=8] {'dp'}, dimensions={0}, use_global_device_ids=true | all-gather | bytes 737280 | tf_op jit(solution)/shard_map/all_gather | solution.py:13
  21.1 0.7 pad_maximum_fusion.1
  21.9 0.8 slice_bitcast_fusion.8
  23.0 45.8 %all-gather.5.cloned.1.call-done = bf16[256,4096]{1,0:T(8,128)(2,1)} async-done(((bf16[16,4096]{1,0:T(8,128)(2,1)}), bf16[256,4096]{1,0:T(8,128)(2,1)}) %all-gather.5.cloned.1.call-update) | async-done | bytes 2097168 | tf_op jit(solution)/shard_map/all_gather | solution.py:13
  68.8 1.9 convolution_convert_fusion.2
  71.4 50.3 %all-gather.9.cloned.1.call-done = bf16[32768,64]{0,1:T(8,128)(2,1)} async-done(((bf16[2048,64]{0,1:T(8,128)(2,1)}), bf16[32768,64]{0,1:T(8,128)(2,1)}) %all-gather.9.cloned.1.call-update) | async-done | bytes 4194320 | tf_op jit(solution)/shard_map/all_gather | solution.py:52
  121.7 4.6 %copy.95 = bf16[8,8,16,2048]{3,2,1,0:T(8,128)(2,1)S(1)} copy(bf16[8,8,16,2048]{3,1,2,0:T(8,128)(2,1)} %bitcast.419) | data formatting | bytes 8388608
  126.3 2.3 copy.75
  128.6 1.6 convolution_convert_fusion.1
  130.5 1.4 pad_maximum_fusion
  132.0 5.3 %all-to-all-start = ((bf16[192,16,192]{0,2,1:T(8,128)(2,1)}), bf16[192,16,192]{0,2,1:T(8,128)(2,1)S(1)}, u32[]{:S(2)}, u32[]{:S(2)}) async-start(bf16[192,16,192]{0,2,1:T(8,128)(2,1)} %pad_maximum_fusion), calls=%async_computation | async-start | bytes 3145728 | tf_op jit(solution)/shard_map/all_to_all | solution.py:29
  138.0 0.8 dynamic_slice.3
  138.9 23.7 %all-to-all-done = bf16[192,16,192]{0,2,1:T(8,128)(2,1)S(1)} async-done(((bf16[192,16,192]{0,2,1:T(8,128)(2,1)}), bf16[192,16,192]{0,2,1:T(8,128)(2,1)S(1)}, u32[]{:S(2)}, u32[]{:S(2)}) %all-to-all-start) | async-done | bytes 1179680 | tf_op jit(solution)/shard_map/all_to_all | solution.py:29
  162.6 0.9 copy.79
  163.5 1.7 all_to_all.27
  165.2 1.6 fusion.120
  166.8 4.8 %fusion.125 = f32[1,512,4,128]{1,2,3,0:T(4,128)S(1)} fusion(f32[1,512,4,128]{1,3,2,0:T(8,128)S(1)} %bitcast.429), kind=kOutput, calls=%fused_computation.159 | output fusion | flops 33292288 | bytes 2097152 | tf_op jit(solution)/shard_map/reduce-window
  171.6 1.3 copy.81
  172.9 2.9 fusion.66
  175.8 5.4 %fusion.74 = f32[1,512,8,128]{1,2,3,0:T(8,128)S(1)} fusion(f32[1,512,8,128]{1,3,2,0:T(8,128)S(1)} %bitcast.424), kind=kOutput, calls=%fused_computation.113 | output fusion | flops 66584576 | bytes 4194304 | tf_op jit(solution)/shard_map/reduce-window.2
  181.2 2.6 copy.83
  183.8 4.1 %fusion.53 = (f32[1,512,1536]{1,2,0:T(8,128)S(1)}, f32[1,512,1536]{1,2,0:T(8,128)}) fusion(s32[512]{0:T(512)S(1)} %iota_add_fusion.3, f32[1536]{0:T(1024)S(1)} %slice_reduce_fusion.1, bf16[3072,1,192]{0,2,1:T(8,128)(2,1)S(1)} %all_to_all.27), kind=kOutput, calls=%fused_computation.82 | convolution fusion | flops 109314048 | bytes 6563840 | tf_op jit(solution)/shard_map/thd,sd->hts/dot_general | solution.py:73
  187.8 10.1 %fusion.42 = f32[1,512,12,128]{1,2,3,0:T(8,128)S(1)} fusion(f32[1,512,12,128]{1,3,2,0:T(8,128)S(1)} %bitcast.422), kind=kOutput, calls=%fused_computation.69 | output fusion | flops 99876864 | bytes 6291456 | tf_op jit(solution)/shard_map/reduce-window.4
  197.9 1.8 copy.85
  199.9 6.1 %fusion.34 = (f32[1,512,2048]{1,2,0:T(8,128)S(1)}, f32[2048,512]{1,0:T(8,128)}) fusion(f32[2048]{0:T(1024)S(1)} %bitcast.439, s32[512]{0:T(512)S(1)} %iota_add_fusion.2, bf16[3072,1,192]{0,2,1:T(8,128)(2,1)} %copy-done.1), kind=kOutput, calls=%fused_computation.56 | convolution fusion | flops 145752064 | bytes 8726528 | tf_op jit(solution)/shard_map/thd,sd->hts/dot_general | solution.py:73
  206.0 10.2 %fusion.40 = f32[1,512,16,128]{1,2,3,0:T(8,128)S(1)} fusion(f32[1,512,16,128]{1,3,2,0:T(8,128)S(1)} %bitcast.421), kind=kOutput, calls=%fused_computation.67 | output fusion | flops 133169152 | bytes 8388608 | tf_op jit(solution)/shard_map/reduce-window.6
  216.2 4.4 %copy.87 = f32[1,512,16,128]{1,3,2,0:T(8,128)} copy(f32[1,512,16,128]{1,2,3,0:T(8,128)S(1)} %fusion.40) | data formatting | bytes 8388608 | tf_op jit(solution)/shard_map/reduce-window.6
  220.7 7.1 %fusion.22 = (f32[1,512,2560]{1,2,0:T(8,128)S(1)}, f32[2560,512,1]{1,0,2:T(8,128)}) fusion(s32[512]{0:T(512)S(1)} %iota_add_fusion.1, f32[2560]{0:T(1024)S(1)} %slice_reduce_fusion, bf16[3072,1,192]{0,2,1:T(8,128)(2,1)} %copy-done.1), kind=kOutput, calls=%fused_computation.38 | convolution fusion | flops 182190080 | bytes 10891264 | tf_op jit(solution)/shard_map/thd,sd->hts/dot_general | solution.py:73
  227.9 15.5 %fusion.14 = f32[1,512,20,128]{1,2,3,0:T(8,128)S(1)} fusion(f32[1,512,20,128]{1,3,2,0:T(8,128)S(1)} %bitcast.418), kind=kOutput, calls=%fused_computation.27 | output fusion | flops 166461440 | bytes 10485760 | tf_op jit(solution)/shard_map/reduce-window.8
  243.4 5.4 %copy.89 = f32[1,512,20,128]{1,3,2,0:T(8,128)} copy(f32[1,512,20,128]{1,2,3,0:T(8,128)S(1)} %fusion.14) | data formatting | bytes 10485760 | tf_op jit(solution)/shard_map/reduce-window.8
  248.9 8.2 %fusion.6 = (f32[1,512,3072]{1,2,0:T(8,128)S(1)}, f32[3072,512]{1,0:T(8,128)}) fusion(f32[3072]{0:T(1024)S(1)} %bitcast.437, s32[512]{0:T(512)S(1)} %iota_add_fusion, bf16[3072,1,192]{0,2,1:T(8,128)(2,1)} %copy-done.1), kind=kOutput, calls=%fused_computation.14 | convolution fusion | flops 218628096 | bytes 13056000 | tf_op jit(solution)/shard_map/thd,sd->hts/dot_general | solution.py:73
  257.1 15.3 %fusion.12 = f32[1,512,24,128]{1,2,3,0:T(8,128)S(1)} fusion(f32[1,512,24,128]{1,3,2,0:T(8,128)S(1)} %bitcast.416), kind=kOutput, calls=%fused_computation.25 | output fusion | flops 199753728 | bytes 12582912 | tf_op jit(solution)/shard_map/reduce-window.10
  272.4 6.3 %copy.91 = f32[1,512,24,128]{1,3,2,0:T(8,128)} copy(f32[1,512,24,128]{1,2,3,0:T(8,128)S(1)} %fusion.12) | data formatting | bytes 12582912 | tf_op jit(solution)/shard_map/reduce-window.10
  278.9 2.6 fusion.118
  281.5 5.8 %fusion.64 = bf16[1,512,1024]{1,2,0:T(8,128)(2,1)S(1)} fusion(f32[1,512,8,128]{1,3,2,0:T(8,128)} %copy.83, f32[1024,512]{1,0:T(8,128)} %get-tuple-element.12, f32[512,8]{0,1:T(8,128)S(1)} %slice_bitcast_fusion.47, f32[1024]{0:T(1024)S(1)} %bitcast.443, s32[512]{0:T(512)S(1)} %iota_add_fusion.4), kind=kLoop, calls=%fused_computation.98 | loop fusion | flops 12582912 | bytes 5265408 | tf_op jit(solution)/shard_map/convert_element_type | solution.py:84
  287.3 6.4 %fusion.51 = bf16[1,512,1536]{1,2,0:T(8,128)(2,1)S(1)} fusion(f32[1,512,12,128]{1,3,2,0:T(8,128)S(1)} %copy.85, f32[1,512,1536]{1,2,0:T(8,128)} %get-tuple-element.14, f32[512,12]{0,1:T(8,128)S(1)} %slice_bitcast_fusion.45, s32[512]{0:T(512)S(1)} %iota_add_fusion.3), kind=kLoop, calls=%fused_computation.80 | loop fusion | flops 17301504 | bytes 7890944 | tf_op jit(solution)/shard_map/convert_element_type | solution.py:84
  293.8 7.3 %fusion.32 = bf16[1,512,2048]{1,2,0:T(8,128)(2,1)S(1)} fusion(f32[1,512,16,128]{1,3,2,0:T(8,128)S(1)} %copy-done, f32[2048,512]{1,0:T(8,128)S(1)} %copy-done.3, f32[512,16]{0,1:T(8,128)S(1)} %slice_bitcast_fusion.43, f32[2048]{0:T(1024)S(1)} %bitcast.440, s32[512]{0:T(512)S(1)} %iota_add_fusion.2), kind=kLoop, calls=%fused_computation.54 | loop fusion | flops 25165824 | bytes 10528768 | tf_op jit(solution)/shard_map/convert_element_type | solution.py:84
  301.1 9.8 %fusion.20 = bf16[1,512,2560]{1,2,0:T(8,128)(2,1)S(1)} fusion(f32[1,512,20,128]{1,3,2,0:T(8,128)S(1)} %bitcast.412, f32[2560,512,1]{1,0,2:T(8,128)} %get-tuple-element.18, f32[512,20]{0,1:T(8,128)S(1)} %slice_bitcast_fusion.41, s32[512]{0:T(512)S(1)} %iota_add_fusion.1), kind=kLoop, calls=%fused_computation.36 | loop fusion | flops 28835840 | bytes 13150208 | tf_op jit(solution)/shard_map/convert_element_type | solution.py:84
  311.1 10.9 %fusion.4 = bf16[1,512,3072]{1,2,0:T(8,128)(2,1)S(1)} fusion(f32[1,512,24,128]{1,3,2,0:T(8,128)S(1)} %bitcast.410, f32[3072,512]{1,0:T(8,128)S(1)} %bitcast.415, f32[512,24]{0,1:T(8,128)S(1)} %slice_bitcast_fusion.39, f32[3072]{0:T(1024)S(1)} %bitcast.438, s32[512]{0:T(512)S(1)} %iota_add_fusion), kind=kLoop, calls=%fused_computation.12 | loop fusion | flops 37748736 | bytes 15792128 | tf_op jit(solution)/shard_map/convert_element_type | solution.py:84
  323.9 0.7 fusion.111
  324.8 0.6 broadcast.282
  325.4 0.9 reduce.5
  327.3 13.3 %all_to_all.33 = bf16[16,2,6144]{2,1,0:T(2,128)(2,1)S(1)} all-to-all(bf16[16,2,6144]{2,1,0:T(2,128)(2,1)S(1)} %reshape.800), channel_id=1, replica_groups=mesh['sp'=16,'dp'=8] {'sp'}, dimensions={0} | all-to-all | bytes 786432 | tf_op jit(solution)/shard_map/all_to_all | solution.py:94
  340.6 0.8 reshape.801
  341.4 1.5 copy.93
  342.9 0.6 all_to_all.29
  343.7 4.1 %fusion.59 = bf16[1,192,2048]{2,1,0:T(8,128)(2,1)} fusion(bf16[192,1024]{0,1:T(8,128)(2,1)S(1)} %bitcast.428, bf16[1024,2048]{1,0:T(8,128)(2,1)} %all-gather.7.cloned.1.call-done), kind=kOutput, calls=%fused_computation.93 | convolution fusion | flops 805699584 | bytes 5373952 | tf_op jit(solution)/shard_map/dot_general | solution.py:96
  (86 shorter events, 6.1 us)
Async XLA Ops:
  6.5 16.2 %copy-start.4 = (bf16[1,192,2048]{2,1,0:T(8,128)(2,1)S(1)}, bf16[1,192,2048]{2,1,0:T(8,128)(2,1)}, u32[]{:S(2)}) copy-start(bf16[1,192,2048]{2,1,0:T(8,128)(2,1)} %param.8) | copy-start | bytes 2359300
  6.5 62.3 %copy-start.7 = (f32[2048]{0:T(1024)S(1)}, f32[2048]{0:T(1024)}, u32[]{:S(2)}) copy-start(f32[2048]{0:T(1024)} %param.9) | copy-start | bytes 24580
  6.5 62.2 %all-gather.5.cloned.1.call-start = ((), (), s32[]{:S(2)}) async-start(), calls=%async_computation.2 | async-start | bytes 2228224 | tf_op jit(solution)/shard_map/all_gather | solution.py:13
  21.8 99.9 %all-gather.9.cloned.1.call-start = ((), (), s32[]{:S(2)}) async-start(), calls=%async_computation.4 | async-start | bytes 4456448 | tf_op jit(solution)/shard_map/all_gather | solution.py:52
  68.8 2.0 copy-start.6
  130.5 7.5 %copy-start.5 = (f32[1,3072,1]{1,2,0:T(1,128)S(1)}, f32[1,3072,1]{1,2,0:T(1,128)}, u32[]{:S(2)}) copy-start(f32[1,3072,1]{1,2,0:T(1,128)} %param.13) | copy-start | bytes 36868
  132.0 30.6 %all-to-all-start = ((bf16[192,16,192]{0,2,1:T(8,128)(2,1)}), bf16[192,16,192]{0,2,1:T(8,128)(2,1)S(1)}, u32[]{:S(2)}, u32[]{:S(2)}) async-start(bf16[192,16,192]{0,2,1:T(8,128)(2,1)} %pad_maximum_fusion), calls=%async_computation | async-start | bytes 3145728 | tf_op jit(solution)/shard_map/all_to_all | solution.py:29
  137.2 206.4 %all-gather.7.cloned.1.call-start = ((), (), s32[]{:S(2)}) async-start(), calls=%async_computation.3 | async-start | bytes 4456448 | tf_op jit(solution)/shard_map/all_gather | solution.py:98
  165.2 18.6 %copy-start.1 = (bf16[3072,1,192]{0,2,1:T(8,128)(2,1)}, bf16[3072,1,192]{0,2,1:T(8,128)(2,1)S(1)}, u32[]{:S(2)}) copy-start(bf16[3072,1,192]{0,2,1:T(8,128)(2,1)S(1)} %all_to_all.27) | copy-start | bytes 3538948
  278.9 14.8 %copy-start.3 = (f32[2048,512]{1,0:T(8,128)S(1)}, f32[2048,512]{1,0:T(8,128)}, u32[]{:S(2)}) copy-start(f32[2048,512]{1,0:T(8,128)} %get-tuple-element.16) | copy-start | bytes 12582916
  281.5 19.6 %slice-start.2 = ((s8[5242880]{0:T(1024)(128)(4,1)}), s8[4194304]{0:T(1024)(128)(4,1)S(1)}, s32[]{:S(2)}) async-start(s8[5242880]{0:T(1024)(128)(4,1)} %bitcast.411), calls=%async_computation.7 | async-start | bytes 8388608
  287.3 6.4 %copy-start = (f32[1,512,16,128]{1,3,2,0:T(8,128)S(1)}, f32[1,512,16,128]{1,3,2,0:T(8,128)}, u32[]{:S(2)}) copy-start(f32[1,512,16,128]{1,3,2,0:T(8,128)} %copy.87) | copy-start | bytes 12582916
  287.3 13.8 %slice-start.3 = ((s8[5242880]{0:T(1024)(128)(4,1)}), s8[1048576]{0:T(1024)(128)(4,1)S(1)}, s32[]{:S(2)}) async-start(s8[5242880]{0:T(1024)(128)(4,1)} %bitcast.411), calls=%async_computation.8 | async-start | bytes 2097152
  293.7 17.3 %slice-start = ((s8[6291456]{0:T(1024)(128)(4,1)}), s8[4194304]{0:T(1024)(128)(4,1)S(1)}, s32[]{:S(2)}) async-start(s8[6291456]{0:T(1024)(128)(4,1)} %bitcast.409), calls=%async_computation.5 | async-start | bytes 8388608
  293.7 17.3 %slice-start.4 = ((s8[6291456]{0:T(1024)(128)(4,1)}), s8[2097152]{0:T(1024)(128)(4,1)S(1)}, s32[]{:S(2)}) async-start(s8[6291456]{0:T(1024)(128)(4,1)} %bitcast.414), calls=%async_computation.9 | async-start | bytes 4194304
  301.1 9.9 %slice-start.1 = ((s8[6291456]{0:T(1024)(128)(4,1)}), s8[2097152]{0:T(1024)(128)(4,1)S(1)}, s32[]{:S(2)}) async-start(s8[6291456]{0:T(1024)(128)(4,1)} %bitcast.409), calls=%async_computation.6 | async-start | bytes 4194304
  301.1 9.9 %slice-start.5 = ((s8[6291456]{0:T(1024)(128)(4,1)}), s8[4194304]{0:T(1024)(128)(4,1)S(1)}, s32[]{:S(2)}) async-start(s8[6291456]{0:T(1024)(128)(4,1)} %bitcast.414), calls=%async_computation.10 | async-start | bytes 8388608
  311.1 10.9 %copy-start.2 = (bf16[3072,1,192]{0,2,1:T(8,128)(2,1)S(1)}, bf16[3072,1,192]{0,2,1:T(8,128)(2,1)}, u32[]{:S(2)}) copy-start(bf16[3072,1,192]{0,2,1:T(8,128)(2,1)} %copy-done.1) | copy-start | bytes 3538948
Sparse Core Ops, SparseCore 0:
  21.9 46.8 all-gather.4
  70.9 50.7 all-gather.8
  140.2 54.9 all-gather.6
